TPU v7x, 256 devices: a 4x2x16 block of a 4x16x16 slice. The times are simulated.
256 devices in a mesh: grp: 2 (over y), fs: 16 (over z), tp: 8 (over x, core).
Axes of the slice: x: 4, y: 2, z: 16, core: 2. Of those that a mesh axis runs over, the one named last changes fastest.
The devices are a block of a 4x16x16 slice.
Arguments:
- tokens: bfloat16 [32768, 2048], P(('grp', 'fs', 'tp')), parts along dimension 0, may hold values from -6 to 6
- norm_gains: float32 [4, 2048], replicated, may hold values from 0.1 to 1.9
- query_weight: bfloat16 [2048, 2048], P('fs', 'tp'), may hold values from -0.125 to 0.125
- key_weight: bfloat16 [2048, 2048], P('fs', 'tp'), may hold values from -0.125 to 0.125
- value_weight: bfloat16 [2048, 4096], P('fs', 'tp'), may hold values from -0.125 to 0.125
- swish_weight: bfloat16 [2048, 4096], P('fs', 'tp'), may hold values from -0.125 to 0.125
- mixer_output: bfloat16 [4096, 2048], P('tp', 'fs'), may hold values from -0.09375 to 0.09375
- gate_weight: bfloat16 [2048, 3072], P('fs', 'tp'), may hold values from -0.125 to 0.125
- up_weight: bfloat16 [2048, 3072], P('fs', 'tp'), may hold values from -0.125 to 0.125
- down_weight: bfloat16 [3072, 2048], P('tp', 'fs'), may hold values from -0.109375 to 0.109375
Outputs:
- layer_output: bfloat16 [32768, 2048], P(('grp', 'fs', 'tp')), parts along dimension 0
There are 2 independent parts, one for each index of `grp`. A program takes and returns all parts, laid end to end along the dimension named above; an argument that names none is the same for every part. Nothing has to cross between parts.
All inputs are finite; a program needn't handle non-finite values.
Results may differ from a plain program's by a relative error of at most 0.02.
Values may be sent and summed in bfloat16 or wider, within the bound.
A program may use at most 64 MiB of HBM per device.

v0:
```python
import jax
import jax.numpy as jnp
from jax import lax
from jax.sharding import PartitionSpec as P

H = 8
QK = 256
BLOCK = 128
norm_epsilon = 1e-06
group_epsilon = 0.01


def laid_out(pieces, dim):
    lengths = list(pieces.shape[1:])
    lengths[dim] *= pieces.shape[0]
    return jnp.moveaxis(pieces, 0, dim).reshape(lengths)


def from_everyone(array, axis):
    copies = jnp.broadcast_to(array, (lax.axis_size(axis), *array.shape))
    return lax.all_to_all(copies, axis, split_axis=0, concat_axis=0, tiled=True)


def gather_directly(array, axis, dim):
    return laid_out(from_everyone(array, axis), dim)


def split_up(array, dim, count):
    before, after = (array.shape[:dim], array.shape[dim + 1 :])
    return jnp.moveaxis(array.reshape(*before, count, -1, *after), dim, 0)


def summed_on_arrival(array, axis, dim):
    count = lax.axis_size(axis)
    pieces = lax.all_to_all(split_up(array, dim, count), axis, 0, 0, tiled=True)
    return jnp.sum(pieces.astype(jnp.float32), axis=0)


def sent_together(arrays, axis, dim, along):
    ends, at = ([], 0)
    for a in arrays[:-1]:
        at += a.shape[along]
        ends.append(at)
    both = jnp.concatenate(arrays, axis=along)
    return tuple(jnp.split(lax.all_gather(both, axis, axis=dim, tiled=True), ends, axis=along))


def rms_scale(matrix, gain):
    return (
        matrix * lax.rsqrt(jnp.mean(matrix * matrix, axis=-1, keepdims=True) + norm_epsilon) * gain
    )


def gather_rows(normed):
    return lax.all_gather(normed, "tp", axis=0, tiled=True)


def add_piece(normed, shard_piece):
    return jnp.dot(normed, shard_piece, preferred_element_type=jnp.float32)


def project_out(active, weight_shard):
    whole_weight = gather_directly(weight_shard, "fs", 1)
    return summed_on_arrival(
        jnp.dot(active, whole_weight, preferred_element_type=jnp.float32).astype(jnp.bfloat16),
        "tp",
        0,
    )


def rotate_halves(head_tensors, cosine_table, sine_table):
    half_width = head_tensors.shape[-1] // 2
    lower_half = head_tensors[..., :half_width]
    upper_half = head_tensors[..., half_width:]
    return jnp.concatenate(
        [
            lower_half * cosine_table - upper_half * sine_table,
            lower_half * sine_table + upper_half * cosine_table,
        ],
        axis=-1,
    )


def retention(queries, key_rows, value_rows, log_decay):
    length, head_count, key_width = queries.shape
    value_width = value_rows.shape[-1]
    blocks = length // BLOCK
    query_blocks = queries.reshape(blocks, BLOCK, head_count, key_width)
    key_blocks = key_rows.reshape(blocks, BLOCK, head_count, key_width)
    value_blocks = value_rows.reshape(blocks, BLOCK, head_count, value_width)
    offsets = jnp.arange(BLOCK, dtype=jnp.float32)
    distance = offsets[:, None] - offsets[None, :]
    within = jnp.where(
        distance >= 0, jnp.exp(log_decay[:, None, None] * jnp.maximum(distance, 0.0)), 0.0
    )
    retention_scores = jnp.einsum(
        "cnhd,cmhd->chnm", query_blocks, key_blocks, preferred_element_type=jnp.float32
    )
    local_part = jnp.einsum(
        "chnm,cmhe->cnhe", retention_scores * within[None], value_blocks.astype(jnp.float32)
    )
    key_decay = jnp.exp((BLOCK - 1.0 - offsets)[:, None] * log_decay[None, :])
    query_decay = jnp.exp((offsets + 1.0)[:, None] * log_decay[None, :])
    block_decay = jnp.exp(BLOCK * log_decay)

    def advance(carry_state, inputs):
        query_block, key_block, value_tile = inputs
        carried = (
            jnp.einsum("nhd,hde->nhe", query_block.astype(jnp.float32), carry_state)
            * query_decay[:, :, None]
        )
        decay_weighted = key_block.astype(jnp.float32) * key_decay[:, :, None]
        carry_state = carry_state * block_decay[:, None, None] + jnp.einsum(
            "yui,yua->uia", decay_weighted, value_tile.astype(jnp.float32)
        )
        return (carry_state, carried)

    starting_state = jnp.zeros((head_count, key_width, value_width), jnp.float32)
    _, carried = lax.scan(advance, starting_state, (query_blocks, key_blocks, value_blocks))
    return (local_part + carried).reshape(length, head_count, value_width)


def per_device(
    tokens,
    norm_gains,
    query_weight,
    key_weight,
    value_weight,
    swish_weight,
    mixer_output,
    gate_weight,
    up_weight,
    down_weight,
):
    residual = tokens.astype(jnp.float32)
    normed = gather_rows(rms_scale(residual, norm_gains[0]).astype(jnp.bfloat16))
    gate_whole, up_whole = sent_together((gate_weight, up_weight), "fs", 0, 1)
    pieces = sent_together((query_weight, key_weight, value_weight, swish_weight), "fs", 0, 1)
    raw_query, raw_keys, raw_values, raw_swish = tuple(
        (add_piece(normed, shard_piece) for shard_piece in pieces)
    )
    length = normed.shape[0]
    head_count = raw_query.shape[1] // QK
    positions = jnp.arange(length, dtype=jnp.float32)
    frequency = 10000.0 ** (-jnp.linspace(0.0, 1.0, QK // 2, dtype=jnp.float32))
    angles = positions[:, None] * frequency[None, :]
    cosine_table = jnp.cos(angles)[:, None, :]
    sine_table = jnp.sin(angles)[:, None, :]
    queries = rotate_halves(
        raw_query.reshape(length, head_count, QK), cosine_table, sine_table
    ).astype(jnp.bfloat16)
    key_rows = (
        rotate_halves(raw_keys.reshape(length, head_count, QK), cosine_table, sine_table)
        * QK ** (-0.5)
    ).astype(jnp.bfloat16)
    value_rows = raw_values.reshape(length, head_count, -1).astype(jnp.bfloat16)
    head_index = (lax.axis_index("tp") * head_count + jnp.arange(head_count)).astype(jnp.float32)
    log_decay = -(4.0 / BLOCK) * (BLOCK / (32.0 * length)) ** (head_index / (H - 1))
    retained = retention(queries, key_rows, value_rows, log_decay)
    centred = retained - jnp.mean(retained, axis=-1, keepdims=True)
    normalized = centred * lax.rsqrt(
        jnp.mean(centred * centred, axis=-1, keepdims=True) + group_epsilon
    )
    gated_rows = (jax.nn.silu(raw_swish) * normalized.reshape(length, -1)).astype(jnp.bfloat16)
    mixer_total = project_out(gated_rows, mixer_output)
    after_mixer = residual + rms_scale(mixer_total, norm_gains[1])
    widened = gather_rows(rms_scale(after_mixer, norm_gains[2]).astype(jnp.bfloat16))
    gate_sum = jnp.dot(widened, gate_whole, preferred_element_type=jnp.float32)
    up_sum = jnp.dot(widened, up_whole, preferred_element_type=jnp.float32)
    hidden = (jax.nn.silu(gate_sum) * up_sum).astype(jnp.bfloat16)
    channel = project_out(hidden, down_weight)
    return (after_mixer + rms_scale(channel, norm_gains[3])).astype(jnp.bfloat16)


def solution(mesh):
    placed = (
        P(("grp", "fs", "tp"), None),
        P(),
        P("fs", "tp"),
        P("fs", "tp"),
        P("fs", "tp"),
        P("fs", "tp"),
        P("tp", "fs"),
        P("fs", "tp"),
        P("fs", "tp"),
        P("tp", "fs"),
    )
    return jax.shard_map(
        per_device,
        mesh=mesh,
        in_specs=placed,
        out_specs=P(("grp", "fs", "tp"), None),
        check_vma=False,
    )
```

profile of v0, /device:TPU:33, one launch (start us, length us, event | category | flops | bytes accessed | tf_op | source)
XLA Modules:
  0.0 461.9 jit_solution(14256166903097563935)
XLA Ops:
  6.6 1.0 fusion.72
  7.6 1.2 fusion.39
  8.8 2.0 fusion.41
  11.0 0.8 pad_maximum_fusion.1
  11.9 0.1 copy.23
  12.0 1.5 broadcast_in_dim.19
  13.5 24.7 %all-to-all-start = ((bf16[16,512,128]{1,2,0:T(8,128)(2,1)}), bf16[16,512,128]{1,2,0:T(8,128)(2,1)}, u32[]{:S(2)}, u32[]{:S(2)}) async-start(bf16[16,512,128]{1,2,0:T(8,128)(2,1)} %broadcast_in_dim.19), calls=%async_computation | async-start | bytes 4194304 | tf_op jit(solution)/shard_map/all_to_all | solution.py:21
  38.3 0.7 pad_maximum_fusion.2
  39.3 0.1 fusion.63
  39.4 24.8 %all-gather.5.cloned.1.call-done = bf16[1024,2048]{1,0:T(8,128)(2,1)} async-done(((bf16[128,2048]{1,0:T(8,128)(2,1)}), bf16[1024,2048]{1,0:T(8,128)(2,1)}) %all-gather.5.cloned.1.call-update) | async-done | bytes 4194320 | tf_op jit(solution)/shard_map/all_gather | solution.py:55
  64.2 130.5 %all-gather.7.cloned.1.call-done = bf16[2048,1536]{1,0:T(8,128)(2,1)} async-done(((bf16[128,1536]{1,0:T(8,128)(2,1)}), bf16[2048,1536]{1,0:T(8,128)(2,1)}) %all-gather.7.cloned.1.call-update) | async-done | bytes 6291472 | tf_op jit(solution)/shard_map/all_gather | solution.py:45
  194.7 3.9 convolution_bitcast_fusion.2
  198.6 0.5 copy-done.10
  199.1 3.4 convolution_bitcast_fusion.3
  202.5 2.3 subtract_convert_fusion
  204.8 0.9 pad_maximum_fusion
  205.7 1.1 fusion.45
  206.8 3.3 fusion.36
  210.1 25.3 %while.15 = (s32[]{:T(128)}, f32[1,256,512]{2,1,0:T(8,128)S(1)}, f32[8,128,1,512]{3,1,2,0:T(8,128)}, f32[1]{0:T(128)}, bf16[8,128,1,256]{3,2,1,0:T(2,128)(2,1)S(...) while((s32[]{:T(128)}, f32[1,256,512]{2,1,0:T(8,128)S(1)}, ...), condition=%wide.region_2.3_spmd.clone.clone.clone, body=%wide.region_1.2_spmd.clone.clone.clone.sunk | while | flops 67797504 | bytes 2232440 | solution.py:119
  210.2 1.7 fusion.99
  211.9 0.2 convert_multiply_fusion.4
  212.1 1.2 fusion.98
  213.3 1.8 fusion.99
  215.1 0.2 convert_multiply_fusion.4
  215.3 1.2 fusion.98
  216.5 1.7 fusion.99
  218.3 0.2 convert_multiply_fusion.4
  218.5 1.2 fusion.98
  219.7 1.7 fusion.99
  221.4 0.2 convert_multiply_fusion.4
  221.6 1.2 fusion.98
  222.8 1.7 fusion.99
  224.6 0.2 convert_multiply_fusion.4
  224.8 1.2 fusion.98
  226.0 1.7 fusion.99
  227.7 0.2 convert_multiply_fusion.4
  228.0 1.2 fusion.98
  229.2 1.8 fusion.99
  230.9 0.2 convert_multiply_fusion.4
  231.1 1.2 fusion.98
  232.3 1.7 fusion.99
  234.1 0.2 convert_multiply_fusion.4
  234.3 1.2 fusion.98
  235.5 2.7 fusion.73
  238.2 0.4 multiply_reduce_fusion
  238.6 5.6 %fusion.27 = bf16[1024,512]{1,0:T(8,128)(2,1)S(1)} fusion(f32[8,128,1,512]{3,1,0,2:T(8,128)S(1)} %get-tuple-element.179, bf16[1024,2048]{1,0:T(8,128)(2,1)} %all-gather.5.cloned.1.call-done, bf16[2048,1536]{1,0:T(8,128)(2,1)} %all-gather.7.cloned.1.call-done, f32[1024]{0:T(1024)S(1)} %rsqrt_bitcast_fusion, f32[1024]{0:T(1024)S(1)} %get-tuple-element.174), kind=kOutput, calls=%fused_computation.36 | convolution fusion | flops 2151677952 | bytes 9445376 | tf_op jit(solution)/shard_map/dot_general | solution.py:59
  244.2 4.0 convolution_convert_fusion.1
  248.2 56.0 %all_to_all.20 = bf16[8,128,2048]{2,1,0:T(8,128)(2,1)S(1)} all-to-all(bf16[8,128,2048]{2,1,0:T(8,128)(2,1)S(1)} %bitcast.130), channel_id=1, replica_groups=mesh['grp'=2,'fs'=16,'tp'=8] {'tp'}, dimensions={0} | all-to-all | bytes 8388608 | tf_op jit(solution)/shard_map/all_to_all | solution.py:35
  304.2 0.7 convert_reduce_fusion.1
  304.9 0.2 multiply_reduce_fusion.3
  305.1 0.2 copy-done
  305.3 0.4 multiply_reduce_fusion.2
  305.6 1.1 multiply_convert_fusion.1
  306.8 0.1 copy.24
  306.9 1.4 broadcast_in_dim.20
  308.3 8.1 %all-to-all-start.2 = ((bf16[16,384,128]{1,2,0:T(8,128)(2,1)}), bf16[16,384,128]{1,2,0:T(8,128)(2,1)S(1)}, u32[]{:S(2)}, u32[]{:S(2)}) async-start(bf16[16,384,128]{1,2,0:T(8,128)(2,1)} %broadcast_in_dim.20), calls=%async_computation.2 | async-start | bytes 3145728 | tf_op jit(solution)/shard_map/all_to_all | solution.py:21
  316.4 25.5 %all-gather.9.cloned.1.call-done = bf16[1024,2048]{1,0:T(8,128)(2,1)} async-done(((bf16[128,2048]{1,0:T(8,128)(2,1)}), bf16[1024,2048]{1,0:T(8,128)(2,1)}) %all-gather.9.cloned.1.call-update) | async-done | bytes 4194320 | tf_op jit(solution)/shard_map/all_gather | solution.py:55
  342.0 6.2 %fusion.30 = f32[1024,384]{1,0:T(8,128)} fusion(bf16[1024,2048]{1,0:T(8,128)(2,1)} %all-gather.9.cloned.1.call-done, bf16[2048,768]{1,0:T(8,128)(2,1)} %all-gather.11.cloned.1.call-done), kind=kOutput, calls=%fused_computation.40 | convolution fusion | flops 1610612736 | bytes 7340032 | tf_op jit(solution)/shard_map/dot_general | solution.py:168
  348.1 37.1 %all-to-all-done.2 = bf16[16,384,128]{1,2,0:T(8,128)(2,1)S(1)} async-done(((bf16[16,384,128]{1,2,0:T(8,128)(2,1)}), bf16[16,384,128]{1,2,0:T(8,128)(2,1)S(1)}, u32[]{:S(2)}, u32[]{:S(2)}) %all-to-all-start.2) | async-done | bytes 1572896 | tf_op jit(solution)/shard_map/all_to_all | solution.py:21
  385.3 9.6 %convolution_convert_fusion = bf16[1024,2048]{1,0:T(8,128)(2,1)} fusion(bf16[384,2048]{0,1:T(8,128)(2,1)S(1)} %bitcast.137, f32[1024,384]{1,0:T(8,128)} %fusion.30, bf16[1024,2048]{1,0:T(8,128)(2,1)} %all-gather.9.cloned.1.call-done, bf16[2048,768]{1,0:T(8,128)(2,1)} %all-gather.11.cloned.1.call-done), kind=kOutput, calls=%fused_computation.26 | convolution fusion | flops 3225681920 | bytes 13107200 | tf_op jit(solution)/shard_map/dot_general | solution.py:65
  394.9 58.4 %all_to_all.21 = bf16[8,128,2048]{2,1,0:T(8,128)(2,1)S(1)} all-to-all(bf16[8,128,2048]{2,1,0:T(8,128)(2,1)} %bitcast.129), channel_id=1, replica_groups=mesh['grp'=2,'fs'=16,'tp'=8] {'tp'}, dimensions={0} | all-to-all | bytes 8388608 | tf_op jit(solution)/shard_map/all_to_all | solution.py:35
  453.2 0.7 convert_reduce_fusion
  454.0 0.2 multiply_reduce_fusion.1
  454.1 1.2 add_convert_fusion
  (50 shorter events, 0.8 us)
Async XLA Ops:
  6.5 4.4 copy-start.9
  6.5 4.5 copy-start.8
  6.6 4.5 copy-start.4
  6.6 4.5 copy-start.3
  6.6 5.3 %copy-start.2 = (bf16[512,128]{1,0:T(8,128)(2,1)S(1)}, bf16[512,128]{1,0:T(8,128)(2,1)}, u32[]{:S(2)}) copy-start(bf16[512,128]{1,0:T(8,128)(2,1)} %param.18) | copy-start | bytes 393220
  6.6 57.6 %all-gather.5.cloned.1.call-start = ((), (), s32[]{:S(2)}) async-start(), calls=%async_computation.4 | async-start | bytes 4718592 | tf_op jit(solution)/shard_map/all_gather | solution.py:55
  10.9 183.8 %all-gather.7.cloned.1.call-start = ((), (), s32[]{:S(2)}) async-start(), calls=%async_computation.5 | async-start | bytes 6684672 | tf_op jit(solution)/shard_map/all_gather | solution.py:45
  13.5 24.7 %copy-start.6 = (bf16[128,384]{1,0:T(8,128)(2,1)S(1)}, bf16[128,384]{1,0:T(8,128)(2,1)}, u32[]{:S(2)}) copy-start(bf16[128,384]{1,0:T(8,128)(2,1)} %param.20) | copy-start | bytes 294916
  13.5 24.7 %copy-start.7 = (bf16[128,384]{1,0:T(8,128)(2,1)S(1)}, bf16[128,384]{1,0:T(8,128)(2,1)}, u32[]{:S(2)}) copy-start(bf16[128,384]{1,0:T(8,128)(2,1)} %param.19) | copy-start | bytes 294916
  13.5 230.7 %all-to-all-start = ((bf16[16,512,128]{1,2,0:T(8,128)(2,1)}), bf16[16,512,128]{1,2,0:T(8,128)(2,1)}, u32[]{:S(2)}, u32[]{:S(2)}) async-start(bf16[16,512,128]{1,2,0:T(8,128)(2,1)} %broadcast_in_dim.19), calls=%async_computation | async-start | bytes 4194304 | tf_op jit(solution)/shard_map/all_to_all | solution.py:21
  38.2 278.3 %all-gather.11.cloned.1.call-start = ((), (), s32[]{:S(2)}) async-start(), calls=%async_computation.7 | async-start | bytes 3342336 | tf_op jit(solution)/shard_map/all_gather | solution.py:45
  39.0 302.9 %all-gather.9.cloned.1.call-start = ((), (), s32[]{:S(2)}) async-start(), calls=%async_computation.6 | async-start | bytes 4718592 | tf_op jit(solution)/shard_map/all_gather | solution.py:55
  194.7 4.4 copy-start.10
  202.5 4.3 copy-start.11
  204.8 5.3 %copy-start.1 = (bf16[1024,1,128]{2,0,1:T(8,128)(2,1)}, bf16[1024,1,128]{2,0,1:T(8,128)(2,1)S(1)}, u32[]{:S(2)}) copy-start(bf16[1024,1,128]{2,0,1:T(8,128)(2,1)S(1)} %get-tuple-element.167) | copy-start | bytes 786436
  304.2 1.0 copy-start
  305.3 1.5 copy-start.5
  308.3 77.0 %all-to-all-start.2 = ((bf16[16,384,128]{1,2,0:T(8,128)(2,1)}), bf16[16,384,128]{1,2,0:T(8,128)(2,1)S(1)}, u32[]{:S(2)}, u32[]{:S(2)}) async-start(bf16[16,384,128]{1,2,0:T(8,128)(2,1)} %broadcast_in_dim.20), calls=%async_computation.2 | async-start | bytes 3145728 | tf_op jit(solution)/shard_map/all_to_all | solution.py:21
Sparse Core Ops, SparseCore 0:
  11.0 53.0 all-gather.4
  66.0 128.6 all-gather.6
  196.5 65.3 all-gather.10
  306.9 34.9 all-gather.8
where the time goes:
time: 463 us; the launch traced here: 462 us
  waiting for transfers between devices  218 us (47%)
  blocking collectives  114 us (25%)
  matrix products  62 us (13%)
  starting transfers between devices  33 us (7%)
  other arithmetic  15.7 us (3%)
  between operations  13.5 us (3%)
  local copies, waits for them, and re-layouts  4.77 us (1%)
    all_gather x2, waiting for transfers between devices, sent_together(): lax.all_gather(both, axis, axis=dim, tiled=True)  131 us
    all_to_all x2, blocking collectives, summed_on_arrival(): pieces = lax.all_to_all(split_up(array, dim, count), axis, 0, 0, tiled=True)  114 us
    all_gather x2, waiting for transfers between devices, gather_rows(): return lax.all_gather(normed, 'tp', axis=0, tiled=True)  50.3 us
    all_to_all x2, waiting for transfers between devices, from_everyone(): return lax.all_to_all(copies, axis, split_axis=0, concat_axis=0, tiled=True)  37.1 us
    all_to_all x2, starting transfers between devices, from_everyone(): return lax.all_to_all(copies, axis, split_axis=0, concat_axis=0, tiled=True)  32.7 us
    dot_general x4, matrix products, add_piece(): return jnp.dot(normed, shard_piece, preferred_element_type=jnp.float32)  16.2 us
    dot_general x8, matrix products, advance(): jnp.einsum('nhd,hde->nhe', query_block.astype(jnp.float32), carry_state)  14 us
    dot_general x2, matrix products, project_out(): jnp.dot(active, whole_weight, preferred_element_type=jnp.float32)  13.6 us
  transfers between devices with their start and end apart: 6, of which 4 were waited for; matrix products, arithmetic and copies ran while one was open for 14% of the time, Pallas kernels for 0%

commit v1 on v0

--- a/solution.py
+++ b/solution.py
@@ -8,6 +8,19 @@
 BLOCK = 128
 norm_epsilon = 1e-06
 group_epsilon = 0.01
+
+
+def collect(x, axis, dim):
+    count, index, span = (lax.axis_size(axis), lax.axis_index(axis), x.shape[dim])
+    right = [(i, (i + 1) % count) for i in range(count)]
+    filled = jnp.zeros((*x.shape[:dim], count * span, *x.shape[dim + 1 :]), x.dtype)
+    block = x
+    for step in range(count):
+        source = (index - step) % count
+        filled = lax.dynamic_update_slice_in_dim(filled, block, source * span, axis=dim)
+        if step < count - 1:
+            block = lax.ppermute(block, axis, right)
+    return filled
 
 
 def laid_out(pieces, dim):
@@ -52,7 +65,7 @@
 
 
 def gather_rows(normed):
-    return lax.all_gather(normed, "tp", axis=0, tiled=True)
+    return collect(normed, "tp", 0)
 
 
 def add_piece(normed, shard_piece):

time: 463 us -> 476 us (1.028)
  blocking collectives: 114 us -> 60.7 us
  waiting for transfers between devices: 218 us -> 247 us
  local copies, waits for them, and re-layouts: 4.77 us -> 22.6 us
  starting transfers between devices: 33 us -> 45.2 us
  matrix products: 62 us -> 67.6 us
    ppermute x0 -> x14, waiting for transfers between devices: none -> 101 us  [collect(): block = lax.ppermute(block, axis, right)]
    all_to_all x2 -> x1, blocking collectives: 114 us -> 60.7 us  [summed_on_arrival(): pieces = lax.all_to_all(split_up(array, dim, count), axis, 0, 0, tiled=True)]
    all_gather x2 -> x0, waiting for transfers between devices: 50.3 us -> none  [gather_rows(): return lax.all_gather(normed, 'tp', axis=0, tiled=True)]
    all_to_all x0 -> x1, waiting for transfers between devices: none -> 47.9 us  [summed_on_arrival(): pieces = lax.all_to_all(split_up(array, dim, count), axis, 0, 0, tiled=True)]
    all_to_all x2, waiting for transfers between devices: 37.1 us -> 0.01 us  [from_everyone(): return lax.all_to_all(copies, axis, split_axis=0, concat_axis=0, tiled=True)]
    all_gather x2, waiting for transfers between devices: 131 us -> 98.2 us  [sent_together(): lax.all_gather(both, axis, axis=dim, tiled=True)]
    ppermute x0 -> x14, starting transfers between devices: none -> 19.1 us  [collect(): block = lax.ppermute(block, axis, right)]
    all_to_all x2, starting transfers between devices: 32.7 us -> 17.3 us  [from_everyone(): return lax.all_to_all(copies, axis, split_axis=0, concat_axis=0, tiled=True)]
  transfers between devices with their start and end apart: 6 -> 19, of which waited for: 4 -> 15; matrix products, arithmetic and copies ran while one was open for 14% -> 19% of each run, Pallas kernels for 0% -> 0%
where the time goes in v1:
time: 476 us; the launch traced here: 475 us
  waiting for transfers between devices  247 us (52%)
  matrix products  67.6 us (14%)
  blocking collectives  60.7 us (13%)
  starting transfers between devices  45.2 us (9%)
  local copies, waits for them, and re-layouts  22.6 us (5%)
  other arithmetic  18.1 us (4%)
  between operations  13.9 us (3%)
    ppermute x14, waiting for transfers between devices, collect(): block = lax.ppermute(block, axis, right)  101 us
    all_gather x2, waiting for transfers between devices, sent_together(): lax.all_gather(both, axis, axis=dim, tiled=True)  98.2 us
    all_to_all x1, blocking collectives, summed_on_arrival(): pieces = lax.all_to_all(split_up(array, dim, count), axis, 0, 0, tiled=True)  60.7 us
    all_to_all x1, waiting for transfers between devices, summed_on_arrival(): pieces = lax.all_to_all(split_up(array, dim, count), axis, 0, 0, tiled=True)  47.9 us
    dot_general x4, matrix products, add_piece(): return jnp.dot(normed, shard_piece, preferred_element_type=jnp.float32)  19.4 us
    ppermute x14, starting transfers between devices, collect(): block = lax.ppermute(block, axis, right)  19.1 us
    all_to_all x2, starting transfers between devices, from_everyone(): return lax.all_to_all(copies, axis, split_axis=0, concat_axis=0, tiled=True)  17.3 us
    dot_general x2, matrix products, project_out(): jnp.dot(active, whole_weight, preferred_element_type=jnp.float32)  15.8 us
  transfers between devices with their start and end apart: 19, of which 15 were waited for; matrix products, arithmetic and copies ran while one was open for 19% of the time, Pallas kernels for 0%

profile of v1, /device:TPU:33, one launch (start us, length us, event | category | flops | bytes accessed | tf_op | source)
XLA Modules:
  0.0 475.2 jit_solution(3221522254193672966)
XLA Ops:
  6.6 1.8 pad_maximum_fusion.1
  8.5 1.2 fusion.37
  10.7 2.6 broadcast.249.clone
  14.2 2.7 collective-permute-start
  16.9 19.1 %collective-permute-done = bf16[128,2048]{1,0:T(8,128)(2,1)S(1)} collective-permute-done((bf16[128,2048]{1,0:T(8,128)(2,1)S(1)}, bf16[128,2048]{1,0:T(8,128)(2,1)S(1)}, u32[]{:S(2)}, u32[]{:S(2)}) %collective-permute-start) | collective-permute-done | bytes 524320 | tf_op jit(solution)/shard_map/ppermute | solution.py:22
  36.0 9.8 %collective-permute-done.1 = bf16[128,2048]{1,0:T(8,128)(2,1)S(1)} collective-permute-done((bf16[128,2048]{1,0:T(8,128)(2,1)S(1)}, bf16[128,2048]{1,0:T(8,128)(2,1)S(1)}, u32[]{:S(2)}, u32[]{:S(2)}) %collective-permute-start.1) | collective-permute-done | bytes 524320 | tf_op jit(solution)/shard_map/ppermute | solution.py:22
  45.9 9.8 %collective-permute-done.2 = bf16[128,2048]{1,0:T(8,128)(2,1)S(1)} collective-permute-done((bf16[128,2048]{1,0:T(8,128)(2,1)S(1)}, bf16[128,2048]{1,0:T(8,128)(2,1)S(1)}, u32[]{:S(2)}, u32[]{:S(2)}) %collective-permute-start.2) | collective-permute-done | bytes 524320 | tf_op jit(solution)/shard_map/ppermute | solution.py:22
  55.7 9.8 %collective-permute-done.3 = bf16[128,2048]{1,0:T(8,128)(2,1)S(1)} collective-permute-done((bf16[128,2048]{1,0:T(8,128)(2,1)S(1)}, bf16[128,2048]{1,0:T(8,128)(2,1)S(1)}, u32[]{:S(2)}, u32[]{:S(2)}) %collective-permute-start.3) | collective-permute-done | bytes 524320 | tf_op jit(solution)/shard_map/ppermute | solution.py:22
  65.6 1.5 broadcast_in_dim.19
  67.2 9.5 %all-to-all-start = ((bf16[16,512,128]{1,2,0:T(8,128)(2,1)}), bf16[16,512,128]{1,2,0:T(8,128)(2,1)}, u32[]{:S(2)}, u32[]{:S(2)}) async-start(bf16[16,512,128]{1,2,0:T(8,128)(2,1)} %broadcast_in_dim.19), calls=%async_computation | async-start | bytes 4194304 | tf_op jit(solution)/shard_map/all_to_all | solution.py:34
  80.0 5.5 %collective-permute-done.5 = bf16[128,2048]{1,0:T(8,128)(2,1)S(1)} collective-permute-done((bf16[128,2048]{1,0:T(8,128)(2,1)}, bf16[128,2048]{1,0:T(8,128)(2,1)S(1)}, u32[]{:S(2)}, u32[]{:S(2)}) %collective-permute-start.5) | collective-permute-done | bytes 524320 | tf_op jit(solution)/shard_map/ppermute | solution.py:22
  87.1 1.9 constant_dynamic-update-slice_fusion.10
  89.9 5.3 %collective-permute-done.6 = bf16[128,2048]{1,0:T(8,128)(2,1)S(1)} collective-permute-done((bf16[128,2048]{1,0:T(8,128)(2,1)S(1)}, bf16[128,2048]{1,0:T(8,128)(2,1)S(1)}, u32[]{:S(2)}, u32[]{:S(2)}) %collective-permute-start.6) | collective-permute-done | bytes 524320 | tf_op jit(solution)/shard_map/ppermute | solution.py:22
  96.1 98.2 %all-gather.3.cloned.1.call-done = bf16[2048,1536]{1,0:T(8,128)(2,1)} async-done(((bf16[128,1536]{1,0:T(8,128)(2,1)}), bf16[2048,1536]{1,0:T(8,128)(2,1)}) %all-gather.3.cloned.1.call-update) | async-done | bytes 6291472 | tf_op jit(solution)/shard_map/all_gather | solution.py:58
  194.3 3.9 convolution_bitcast_fusion.2
  198.7 3.4 convolution_bitcast_fusion.3
  202.2 2.3 subtract_convert_fusion
  205.4 1.1 fusion.43
  206.5 5.5 %fusion.34 = bf16[1024,512]{1,0:T(8,128)(2,1)} fusion(bf16[1024,2048]{1,0:T(8,128)(2,1)} %constant_dynamic-update-slice_fusion.8, bf16[2048,1536]{1,0:T(8,128)(2,1)S(1)} %copy-done.7), kind=kOutput, calls=%fused_computation.46 | convolution fusion | flops 2148007936 | bytes 7340032 | tf_op jit(solution)/shard_map/dot_general | solution.py:72
  212.0 25.3 %while.15 = (s32[]{:T(128)}, f32[1,256,512]{2,1,0:T(8,128)S(1)}, f32[8,128,1,512]{3,1,2,0:T(8,128)}, f32[1]{0:T(128)}, bf16[8,128,1,256]{3,2,1,0:T(2,128)(2,1)S(...) while((s32[]{:T(128)}, f32[1,256,512]{2,1,0:T(8,128)S(1)}, ...), condition=%wide.region_2.3_spmd.clone.clone.clone, body=%wide.region_1.2_spmd.clone.clone.clone.sunk | while | flops 67797504 | bytes 2232440 | solution.py:132
  212.1 1.8 fusion.100
  214.0 1.2 fusion.99
  215.2 1.7 fusion.100
  217.2 1.2 fusion.99
  218.4 1.8 fusion.100
  220.4 1.2 fusion.99
  221.6 1.7 fusion.100
  223.5 1.2 fusion.99
  224.7 1.7 fusion.100
  226.7 1.2 fusion.99
  227.9 1.7 fusion.100
  229.8 1.2 fusion.99
  231.1 1.8 fusion.100
  233.0 1.2 fusion.99
  234.2 1.7 fusion.100
  236.2 1.2 fusion.99
  237.4 2.8 fusion.74
  240.6 6.5 %fusion.27 = bf16[1024,512]{1,0:T(8,128)(2,1)} fusion(f32[8,128,1,512]{3,1,0,2:T(8,128)S(1)} %get-tuple-element.183, bf16[1024,2048]{1,0:T(8,128)(2,1)} %constant_dynamic-update-slice_fusion.8, bf16[2048,1536]{1,0:T(8,128)(2,1)} %all-gather.3.cloned.1.call-done, f32[1024]{0:T(1024)S(1)} %rsqrt_bitcast_fusion, f32[1024]{0:T(1024)S(1)} %get-tuple-element.178), kind=kOutput, calls=%fused_computation.36 | convolution fusion | flops 2151677952 | bytes 9445376 | tf_op jit(solution)/shard_map/dot_general | solution.py:72
  247.2 6.2 %convolution_convert_fusion.1 = bf16[1024,2048]{1,0:T(8,128)(2,1)} fusion(bf16[1024,512]{1,0:T(8,128)(2,1)} %fusion.27, bf16[512,2048]{0,1:T(8,128)(2,1)} %bitcast.26), kind=kOutput, calls=%fused_computation.27 | convolution fusion | flops 2149580800 | bytes 7340032 | tf_op jit(solution)/shard_map/dot_general | solution.py:78
  253.4 8.8 %all-to-all-start.1 = ((bf16[8,128,2048]{2,1,0:T(8,128)(2,1)}), bf16[8,128,2048]{2,1,0:T(8,128)(2,1)}, u32[]{:S(2)}, u32[]{:S(2)}) async-start(bf16[8,128,2048]{2,1,0:T(8,128)(2,1)} %bitcast.129), calls=%async_computation.1 | async-start | bytes 8388608 | tf_op jit(solution)/shard_map/all_to_all | solution.py:48
  263.1 47.9 %all-to-all-done.1 = bf16[8,128,2048]{2,1,0:T(8,128)(2,1)} async-done(((bf16[8,128,2048]{2,1,0:T(8,128)(2,1)}), bf16[8,128,2048]{2,1,0:T(8,128)(2,1)}, u32[]{:S(2)}, u32[]{:S(2)}) %all-to-all-start.1) | async-done | bytes 4194336 | tf_op jit(solution)/shard_map/all_to_all | solution.py:48
  311.0 1.4 broadcast_in_dim.20
  312.3 7.8 %all-to-all-start.2 = ((bf16[16,384,128]{1,2,0:T(8,128)(2,1)}), bf16[16,384,128]{1,2,0:T(8,128)(2,1)S(1)}, u32[]{:S(2)}, u32[]{:S(2)}) async-start(bf16[16,384,128]{1,2,0:T(8,128)(2,1)} %broadcast_in_dim.20), calls=%async_computation.2 | async-start | bytes 3145728 | tf_op jit(solution)/shard_map/all_to_all | solution.py:34
  320.1 3.0 convert_reduce_fusion.1
  323.7 2.5 broadcast.249
  326.2 1.1 constant_dynamic-update-slice_fusion.7
  327.3 1.5 collective-permute-start.7
  328.8 6.1 %collective-permute-done.7 = bf16[128,2048]{1,0:T(8,128)(2,1)S(1)} collective-permute-done((bf16[128,2048]{1,0:T(8,128)(2,1)S(1)}, bf16[128,2048]{1,0:T(8,128)(2,1)S(1)}, u32[]{:S(2)}, u32[]{:S(2)}) %collective-permute-start.7) | collective-permute-done | bytes 524320 | tf_op jit(solution)/shard_map/ppermute | solution.py:22
  334.9 2.5 collective-permute-start.8
  337.4 6.1 %collective-permute-done.8 = bf16[128,2048]{1,0:T(8,128)(2,1)S(1)} collective-permute-done((bf16[128,2048]{1,0:T(8,128)(2,1)S(1)}, bf16[128,2048]{1,0:T(8,128)(2,1)S(1)}, u32[]{:S(2)}, u32[]{:S(2)}) %collective-permute-start.8) | collective-permute-done | bytes 524320 | tf_op jit(solution)/shard_map/ppermute | solution.py:22
  343.5 2.5 collective-permute-start.9
  346.0 6.1 %collective-permute-done.9 = bf16[128,2048]{1,0:T(8,128)(2,1)S(1)} collective-permute-done((bf16[128,2048]{1,0:T(8,128)(2,1)S(1)}, bf16[128,2048]{1,0:T(8,128)(2,1)S(1)}, u32[]{:S(2)}, u32[]{:S(2)}) %collective-permute-start.9) | collective-permute-done | bytes 524320 | tf_op jit(solution)/shard_map/ppermute | solution.py:22
  352.1 2.5 collective-permute-start.10
  354.6 6.1 %collective-permute-done.10 = bf16[128,2048]{1,0:T(8,128)(2,1)S(1)} collective-permute-done((bf16[128,2048]{1,0:T(8,128)(2,1)S(1)}, bf16[128,2048]{1,0:T(8,128)(2,1)S(1)}, u32[]{:S(2)}, u32[]{:S(2)}) %collective-permute-start.10) | collective-permute-done | bytes 524320 | tf_op jit(solution)/shard_map/ppermute | solution.py:22
  360.7 2.5 collective-permute-start.11
  363.2 6.1 %collective-permute-done.11 = bf16[128,2048]{1,0:T(8,128)(2,1)S(1)} collective-permute-done((bf16[128,2048]{1,0:T(8,128)(2,1)S(1)}, bf16[128,2048]{1,0:T(8,128)(2,1)S(1)}, u32[]{:S(2)}, u32[]{:S(2)}) %collective-permute-start.11) | collective-permute-done | bytes 524320 | tf_op jit(solution)/shard_map/ppermute | solution.py:22
  369.4 2.5 collective-permute-start.12
  374.4 4.7 collective-permute-done.12
  379.0 1.4 collective-permute-start.13
  382.9 5.9 %collective-permute-done.13 = bf16[128,2048]{1,0:T(8,128)(2,1)S(1)} collective-permute-done((bf16[128,2048]{1,0:T(8,128)(2,1)S(1)}, bf16[128,2048]{1,0:T(8,128)(2,1)S(1)}, u32[]{:S(2)}, u32[]{:S(2)}) %collective-permute-start.13) | collective-permute-done | bytes 524320 | tf_op jit(solution)/shard_map/ppermute | solution.py:22
  389.7 6.2 %fusion.28 = f32[1024,384]{1,0:T(8,128)} fusion(bf16[1024,2048]{1,0:T(8,128)(2,1)} %constant_dynamic-update-slice_fusion, bf16[2048,768]{1,0:T(8,128)(2,1)} %all-gather.5.cloned.1.call-done), kind=kOutput, calls=%fused_computation.38 | convolution fusion | flops 1610612736 | bytes 7340032 | tf_op jit(solution)/shard_map/dot_general | solution.py:182
  396.0 9.6 %convolution_convert_fusion = bf16[1024,2048]{1,0:T(8,128)(2,1)} fusion(bf16[384,2048]{0,1:T(8,128)(2,1)S(1)} %bitcast.137, f32[1024,384]{1,0:T(8,128)} %fusion.28, bf16[1024,2048]{1,0:T(8,128)(2,1)} %constant_dynamic-update-slice_fusion, bf16[2048,768]{1,0:T(8,128)(2,1)} %all-gather.5.cloned.1.call-done), kind=kOutput, calls=%fused_computation.26 | convolution fusion | flops 3225681920 | bytes 13107200 | tf_op jit(solution)/shard_map/dot_general | solution.py:78
  405.6 60.7 %all_to_all.20 = bf16[8,128,2048]{2,1,0:T(8,128)(2,1)S(1)} all-to-all(bf16[8,128,2048]{2,1,0:T(8,128)(2,1)} %bitcast.130), channel_id=1, replica_groups=mesh['grp'=2,'fs'=16,'tp'=8] {'tp'}, dimensions={0} | all-to-all | bytes 8388608 | tf_op jit(solution)/shard_map/all_to_all | solution.py:48
  467.2 1.2 add_convert_fusion
  (81 shorter events, 20.3 us)
Async XLA Ops:
  6.5 6.7 %copy-start = (bf16[128,2048]{1,0:T(8,128)(2,1)S(1)}, bf16[128,2048]{1,0:T(8,128)(2,1)}, u32[]{:S(2)}) copy-start(bf16[128,2048]{1,0:T(8,128)(2,1)} %param.12) | copy-start | bytes 1572868
  6.5 58.9 %copy-start.3 = (bf16[512,128]{1,0:T(8,128)(2,1)S(1)}, bf16[512,128]{1,0:T(8,128)(2,1)}, u32[]{:S(2)}) copy-start(bf16[512,128]{1,0:T(8,128)(2,1)} %param.18) | copy-start | bytes 393220
  6.6 187.8 %all-gather.3.cloned.1.call-start = ((), (), s32[]{:S(2)}) async-start(), calls=%async_computation.4 | async-start | bytes 6684672 | tf_op jit(solution)/shard_map/all_gather | solution.py:58
  14.2 21.8 %collective-permute-start = (bf16[128,2048]{1,0:T(8,128)(2,1)S(1)}, bf16[128,2048]{1,0:T(8,128)(2,1)S(1)}, u32[]{:S(2)}, u32[]{:S(2)}) collective-permute-start(bf16[128,2048]{1,0:T(8,128)(2,1)S(1)} %get-tuple-element.167), channel_id=1, source_target_pairs={{0,1},{1,2},{2,3},{3,4},{4,5},{5,6},{6,7},{7,0},{8,9},{9,10},{10,1... | collective-permute-start | bytes 1572872 | tf_op jit(solution)/shard_map/ppermute | solution.py:22
  36.0 9.8 %collective-permute-start.1 = (bf16[128,2048]{1,0:T(8,128)(2,1)S(1)}, bf16[128,2048]{1,0:T(8,128)(2,1)S(1)}, u32[]{:S(2)}, u32[]{:S(2)}) collective-permute-start(bf16[128,2048]{1,0:T(8,128)(2,1)S(1)} %collective-permute-done), channel_id=1, source_target_pairs={{0,1},{1,2},{2,3},{3,4},{4,5},{5,6},{6,7},{7,0},{8,9},{9,10},{10,1... | collective-permute-start | bytes 1572872 | tf_op jit(solution)/shard_map/ppermute | solution.py:22
  45.9 9.8 %collective-permute-start.2 = (bf16[128,2048]{1,0:T(8,128)(2,1)S(1)}, bf16[128,2048]{1,0:T(8,128)(2,1)S(1)}, u32[]{:S(2)}, u32[]{:S(2)}) collective-permute-start(bf16[128,2048]{1,0:T(8,128)(2,1)S(1)} %collective-permute-done.1), channel_id=1, source_target_pairs={{0,1},{1,2},{2,3},{3,4},{4,5},{5,6},{6,7},{7,0},{8,9},{9,10},{10,1... | collective-permute-start | bytes 1572872 | tf_op jit(solution)/shard_map/ppermute | solution.py:22
  55.7 9.8 %collective-permute-start.3 = (bf16[128,2048]{1,0:T(8,128)(2,1)S(1)}, bf16[128,2048]{1,0:T(8,128)(2,1)S(1)}, u32[]{:S(2)}, u32[]{:S(2)}) collective-permute-start(bf16[128,2048]{1,0:T(8,128)(2,1)S(1)} %collective-permute-done.2), channel_id=1, source_target_pairs={{0,1},{1,2},{2,3},{3,4},{4,5},{5,6},{6,7},{7,0},{8,9},{9,10},{10,1... | collective-permute-start | bytes 1572872 | tf_op jit(solution)/shard_map/ppermute | solution.py:22
  65.5 11.6 %collective-permute-start.4 = (bf16[128,2048]{1,0:T(8,128)(2,1)S(1)}, bf16[128,2048]{1,0:T(8,128)(2,1)}, u32[]{:S(2)}, u32[]{:S(2)}) collective-permute-start(bf16[128,2048]{1,0:T(8,128)(2,1)S(1)} %collective-permute-done.3), channel_id=1, source_target_pairs={{0,1},{1,2},{2,3},{3,4},{4,5},{5,6},{6,7},{7,0},{8,9},{9,10},{10,1... | collective-permute-start | bytes 1572872 | tf_op jit(solution)/shard_map/ppermute | solution.py:22
  67.2 180.0 %all-to-all-start = ((bf16[16,512,128]{1,2,0:T(8,128)(2,1)}), bf16[16,512,128]{1,2,0:T(8,128)(2,1)}, u32[]{:S(2)}, u32[]{:S(2)}) async-start(bf16[16,512,128]{1,2,0:T(8,128)(2,1)} %broadcast_in_dim.19), calls=%async_computation | async-start | bytes 4194304 | tf_op jit(solution)/shard_map/all_to_all | solution.py:34
  77.1 8.3 %collective-permute-start.5 = (bf16[128,2048]{1,0:T(8,128)(2,1)}, bf16[128,2048]{1,0:T(8,128)(2,1)S(1)}, u32[]{:S(2)}, u32[]{:S(2)}) collective-permute-start(bf16[128,2048]{1,0:T(8,128)(2,1)} %collective-permute-done.4), channel_id=1, source_target_pairs={{0,1},{1,2},{2,3},{3,4},{4,5},{5,6},{6,7},{7,0},{8,9},{9,10},{10,1... | collective-permute-start | bytes 1572872 | tf_op jit(solution)/shard_map/ppermute | solution.py:22
  85.4 9.8 %collective-permute-start.6 = (bf16[128,2048]{1,0:T(8,128)(2,1)S(1)}, bf16[128,2048]{1,0:T(8,128)(2,1)S(1)}, u32[]{:S(2)}, u32[]{:S(2)}) collective-permute-start(bf16[128,2048]{1,0:T(8,128)(2,1)S(1)} %collective-permute-done.5), channel_id=1, source_target_pairs={{0,1},{1,2},{2,3},{3,4},{4,5},{5,6},{6,7},{7,0},{8,9},{9,10},{10,1... | collective-permute-start | bytes 1572872 | tf_op jit(solution)/shard_map/ppermute | solution.py:22
  194.3 4.4 copy-start.7
  204.4 1.0 copy-start.2
  204.4 7.6 %copy-start.1 = (f32[1024,1,128]{2,0,1:T(8,128)}, f32[1024,1,128]{2,0,1:T(8,128)S(1)}, u32[]{:S(2)}) copy-start(f32[1024,1,128]{2,0,1:T(8,128)S(1)} %get-tuple-element.181) | copy-start | bytes 1572868
  253.4 8.8 %copy-start.5 = (bf16[128,384]{1,0:T(8,128)(2,1)S(1)}, bf16[128,384]{1,0:T(8,128)(2,1)}, u32[]{:S(2)}) copy-start(bf16[128,384]{1,0:T(8,128)(2,1)} %param.20) | copy-start | bytes 294916
  253.4 8.8 %copy-start.6 = (bf16[128,384]{1,0:T(8,128)(2,1)S(1)}, bf16[128,384]{1,0:T(8,128)(2,1)}, u32[]{:S(2)}) copy-start(bf16[128,384]{1,0:T(8,128)(2,1)} %param.19) | copy-start | bytes 294916
  253.4 9.5 %copy-start.4 = (bf16[384,128]{1,0:T(8,128)(2,1)S(1)}, bf16[384,128]{1,0:T(8,128)(2,1)}, u32[]{:S(2)}) copy-start(bf16[384,128]{1,0:T(8,128)(2,1)} %param.21) | copy-start | bytes 294916
  253.4 57.5 %all-to-all-start.1 = ((bf16[8,128,2048]{2,1,0:T(8,128)(2,1)}), bf16[8,128,2048]{2,1,0:T(8,128)(2,1)}, u32[]{:S(2)}, u32[]{:S(2)}) async-start(bf16[8,128,2048]{2,1,0:T(8,128)(2,1)} %bitcast.129), calls=%async_computation.1 | async-start | bytes 8388608 | tf_op jit(solution)/shard_map/all_to_all | solution.py:48
  262.2 127.6 %all-gather.5.cloned.1.call-start = ((), (), s32[]{:S(2)}) async-start(), calls=%async_computation.5 | async-start | bytes 3342336 | tf_op jit(solution)/shard_map/all_gather | solution.py:58
  312.3 83.7 %all-to-all-start.2 = ((bf16[16,384,128]{1,2,0:T(8,128)(2,1)}), bf16[16,384,128]{1,2,0:T(8,128)(2,1)S(1)}, u32[]{:S(2)}, u32[]{:S(2)}) async-start(bf16[16,384,128]{1,2,0:T(8,128)(2,1)} %broadcast_in_dim.20), calls=%async_computation.2 | async-start | bytes 3145728 | tf_op jit(solution)/shard_map/all_to_all | solution.py:34
  327.3 7.6 %collective-permute-start.7 = (bf16[128,2048]{1,0:T(8,128)(2,1)S(1)}, bf16[128,2048]{1,0:T(8,128)(2,1)S(1)}, u32[]{:S(2)}, u32[]{:S(2)}) collective-permute-start(bf16[128,2048]{1,0:T(8,128)(2,1)S(1)} %get-tuple-element.165), channel_id=1, source_target_pairs={{0,1},{1,2},{2,3},{3,4},{4,5},{5,6},{6,7},{7,0},{8,9},{9,10},{10,1... | collective-permute-start | bytes 1572872 | tf_op jit(solution)/shard_map/ppermute | solution.py:22
  334.9 8.6 %collective-permute-start.8 = (bf16[128,2048]{1,0:T(8,128)(2,1)S(1)}, bf16[128,2048]{1,0:T(8,128)(2,1)S(1)}, u32[]{:S(2)}, u32[]{:S(2)}) collective-permute-start(bf16[128,2048]{1,0:T(8,128)(2,1)S(1)} %collective-permute-done.7), channel_id=1, source_target_pairs={{0,1},{1,2},{2,3},{3,4},{4,5},{5,6},{6,7},{7,0},{8,9},{9,10},{10,1... | collective-permute-start | bytes 1572872 | tf_op jit(solution)/shard_map/ppermute | solution.py:22
  343.5 8.6 %collective-permute-start.9 = (bf16[128,2048]{1,0:T(8,128)(2,1)S(1)}, bf16[128,2048]{1,0:T(8,128)(2,1)S(1)}, u32[]{:S(2)}, u32[]{:S(2)}) collective-permute-start(bf16[128,2048]{1,0:T(8,128)(2,1)S(1)} %collective-permute-done.8), channel_id=1, source_target_pairs={{0,1},{1,2},{2,3},{3,4},{4,5},{5,6},{6,7},{7,0},{8,9},{9,10},{10,1... | collective-permute-start | bytes 1572872 | tf_op jit(solution)/shard_map/ppermute | solution.py:22
  352.1 8.6 %collective-permute-start.10 = (bf16[128,2048]{1,0:T(8,128)(2,1)S(1)}, bf16[128,2048]{1,0:T(8,128)(2,1)S(1)}, u32[]{:S(2)}, u32[]{:S(2)}) collective-permute-start(bf16[128,2048]{1,0:T(8,128)(2,1)S(1)} %collective-permute-done.9), channel_id=1, source_target_pairs={{0,1},{1,2},{2,3},{3,4},{4,5},{5,6},{6,7},{7,0},{8,9},{9,10},{10,1... | collective-permute-start | bytes 1572872 | tf_op jit(solution)/shard_map/ppermute | solution.py:22
  360.7 8.6 %collective-permute-start.11 = (bf16[128,2048]{1,0:T(8,128)(2,1)S(1)}, bf16[128,2048]{1,0:T(8,128)(2,1)S(1)}, u32[]{:S(2)}, u32[]{:S(2)}) collective-permute-start(bf16[128,2048]{1,0:T(8,128)(2,1)S(1)} %collective-permute-done.10), channel_id=1, source_target_pairs={{0,1},{1,2},{2,3},{3,4},{4,5},{5,6},{6,7},{7,0},{8,9},{9,10},{10,1... | collective-permute-start | bytes 1572872 | tf_op jit(solution)/shard_map/ppermute | solution.py:22
  369.4 9.7 %collective-permute-start.12 = (bf16[128,2048]{1,0:T(8,128)(2,1)S(1)}, bf16[128,2048]{1,0:T(8,128)(2,1)S(1)}, u32[]{:S(2)}, u32[]{:S(2)}) collective-permute-start(bf16[128,2048]{1,0:T(8,128)(2,1)S(1)} %collective-permute-done.11), channel_id=1, source_target_pairs={{0,1},{1,2},{2,3},{3,4},{4,5},{5,6},{6,7},{7,0},{8,9},{9,10},{10,1... | collective-permute-start | bytes 1572872 | tf_op jit(solution)/shard_map/ppermute | solution.py:22
  379.0 9.8 %collective-permute-start.13 = (bf16[128,2048]{1,0:T(8,128)(2,1)S(1)}, bf16[128,2048]{1,0:T(8,128)(2,1)S(1)}, u32[]{:S(2)}, u32[]{:S(2)}) collective-permute-start(bf16[128,2048]{1,0:T(8,128)(2,1)S(1)} %collective-permute-done.12), channel_id=1, source_target_pairs={{0,1},{1,2},{2,3},{3,4},{4,5},{5,6},{6,7},{7,0},{8,9},{9,10},{10,1... | collective-permute-start | bytes 1572872 | tf_op jit(solution)/shard_map/ppermute | solution.py:22
Sparse Core Ops, SparseCore 0:
  9.2 185.1 all-gather.2
  264.8 73.3 all-gather.4
